TPU v7x, 32 devices: a whole 2x2x4 slice. The times are simulated.
32 devices in a mesh: ep: 8 (over z, core), tp: 4 (over y, x).
Axes of the slice: x: 2, y: 2, z: 4, core: 2. Of those that a mesh axis runs over, the one named last changes fastest.
Arguments:
- tokens: bfloat16 [512, 2048], P('ep'), may hold values from -6 to 6
- mix_gain: float32 [2048], replicated, may hold values from 0.1 to 1.9
- w_in: bfloat16 [2048, 1024], P(None, 'tp'), may hold values from -0.125 to 0.125
- decay_re: float32 [64, 64], P('tp'), may hold values from -1 to -0.1
- freq: float32 [64, 64], P('tp'), may hold values from 0 to 100
- log_step: float32 [64], P('tp'), may hold values from -3.9 to 0
- in_re: bfloat16 [64, 16, 64], P('tp'), may hold values from -1 to 1
- in_im: bfloat16 [64, 16, 64], P('tp'), may hold values from -1 to 1
- out_re: bfloat16 [64, 16, 64], P('tp'), may hold values from -0.75 to 0.75
- out_im: bfloat16 [64, 16, 64], P('tp'), may hold values from -0.75 to 0.75
- skip: float32 [64, 16], P('tp'), may hold values from -4 to 4
- state_re: float32 [512, 64, 64], P('ep', 'tp'), may hold values from -6 to 6
- state_im: float32 [512, 64, 64], P('ep', 'tp'), may hold values from -6 to 6
- glu_weight: bfloat16 [1024, 1024], P(None, 'tp'), may hold values from -0.1875 to 0.1875
- glu_bias: float32 [1024], P('tp'), may hold values from -4 to 4
- out_weight: bfloat16 [1024, 2048], P('tp'), may hold values from -0.1875 to 0.1875
- ffn_gain: float32 [2048], replicated, may hold values from 0.1 to 1.9
- route: int32 [512, 2], P('ep'), may hold values from 0 to 7, all different within a row; in each aligned block of 64 rows (0 to 63, 64 to 127, ...) at most 24 rows name the same one
- route_weight: float32 [512, 2], P('ep'), may hold values from 0.2 to 1
- expert_gate: bfloat16 [8, 2048, 3584], P('ep', None, 'tp'), may hold values from -0.125 to 0.125
- expert_up: bfloat16 [8, 2048, 3584], P('ep', None, 'tp'), may hold values from -0.125 to 0.125
- expert_down: bfloat16 [8, 3584, 2048], P('ep', 'tp'), may hold values from -0.09375 to 0.09375
Outputs:
- mixed: bfloat16 [512, 2048], P('ep', 'tp')
- new_re: float32 [512, 64, 64], P('ep', 'tp')
- new_im: float32 [512, 64, 64], P('ep', 'tp')
Inputs may be any that keep to these rules, and one draw needn't show every extreme that they name: `route`: each row names 2 different experts. Within the 64 rows of one index of ep no expert is named more than 24 times, and in every draw some expert is named exactly 24 times by the rows of some index of ep.
All inputs are finite; a program needn't handle non-finite values.
Results may differ from a plain program's by a relative error of at most 0.015.
Values may be sent and summed in bfloat16 or wider, within the bound.
A program may use at most 64 MiB of HBM per device.

v0:
```python
import functools
import jax
import jax.numpy as jnp
from jax import lax
from jax.experimental import pallas as pl
from jax.experimental.pallas import tpu as pltpu
from jax.sharding import PartitionSpec as P

norm_eps = 1e-06
MESH = pl.DeviceIdType.MESH


def rms_scale(rows, gain):
    values = rows.astype(jnp.float32)
    scaled = values * lax.rsqrt(jnp.mean(values * values, axis=-1, keepdims=True) + norm_eps)
    return (scaled * gain).astype(jnp.bfloat16)


def state_kernel(
    tokens_ref,
    mix_gain_ref,
    w_in_ref,
    decay_ref,
    freq_ref,
    log_step_ref,
    in_re_ref,
    in_im_ref,
    out_re_ref,
    out_im_ref,
    skip_ref,
    state_re_hbm,
    state_im_hbm,
    mixed_ref,
    new_re_hbm,
    new_im_hbm,
    state_re,
    state_im,
    state_sem,
    new_sem,
):
    f32 = jnp.float32
    bf16 = jnp.bfloat16
    groups, places, entries = in_re_ref.shape
    seqs, chan = mixed_ref.shape

    @pl.loop(0, groups)
    def _(g):
        for i, (far, near) in enumerate(((state_re_hbm, state_re), (state_im_hbm, state_im))):
            pltpu.make_async_copy(far.at[:, g, :], near.at[g], state_sem.at[i]).start()

    diagonal = lax.broadcasted_iota(jnp.int32, (groups, groups), 0)
    diagonal = diagonal == lax.broadcasted_iota(jnp.int32, (groups, groups), 1)
    log_step = jnp.sum(jnp.where(diagonal, log_step_ref[...], 0.0), axis=1, keepdims=True)
    step = jnp.exp(log_step)
    decay = decay_ref[...]
    freq = freq_ref[...]
    magnitude = jnp.exp(decay * step)
    turn_re = magnitude * jnp.cos(freq * step)
    turn_im = magnitude * jnp.sin(freq * step)
    denom = decay * decay + freq * freq
    coef_re = ((turn_re - 1.0) * decay + turn_im * freq) / denom
    coef_im = (turn_im * decay - (turn_re - 1.0) * freq) / denom

    def lane_group(shape):
        lane = lax.broadcasted_iota(jnp.int32, shape, len(shape) - 1)
        first = lax.broadcasted_iota(jnp.int32, shape, 0) * places
        return (lane >= first) & (lane < first + places)

    spread = lax.broadcasted_iota(jnp.int32, (places, chan), 1) % places
    spread = spread == lax.broadcasted_iota(jnp.int32, (places, chan), 0)
    skip = jnp.dot(
        skip_ref[...],
        spread.astype(f32),
        precision=lax.Precision.HIGHEST,
        preferred_element_type=f32,
    )
    skip = jnp.sum(jnp.where(lane_group((groups, chan)), skip, 0.0), axis=0, keepdims=True)

    normed = rms_scale(tokens_ref[...], mix_gain_ref[...])
    drive = jnp.dot(normed, w_in_ref[...], preferred_element_type=f32).astype(bf16)
    own_group = lane_group((groups, seqs, chan))
    apart = jnp.where(own_group, drive.astype(f32)[None], 0.0).astype(bf16)
    apart = apart.reshape(groups * seqs, chan)

    def driven(ref):
        weight = ref[...].astype(f32).reshape(chan, entries).astype(bf16)
        value = jnp.dot(apart, weight, preferred_element_type=f32)
        return value.reshape(groups, seqs, entries)

    drive_re, drive_im = driven(in_re_ref), driven(in_im_ref)
    turn_re, turn_im = turn_re[:, None, :], turn_im[:, None, :]
    coef_re, coef_im = coef_re[:, None, :], coef_im[:, None, :]
    drain(state_re, state_sem.at[0])
    drain(state_im, state_sem.at[1])
    old_re, old_im = state_re[...], state_im[...]
    new_re = turn_re * old_re - turn_im * old_im + (coef_re * drive_re - coef_im * drive_im)
    new_im = turn_re * old_im + turn_im * old_re + (coef_re * drive_im + coef_im * drive_re)
    state_re[...] = new_re
    state_im[...] = new_im

    @pl.loop(0, groups)
    def _(g):
        for i, (near, far) in enumerate(((state_re, new_re_hbm), (state_im, new_im_hbm))):
            pltpu.make_async_copy(near.at[g], far.at[:, g, :], new_sem.at[i]).start()

    def read_out(value, ref):
        weight = ref[...].astype(f32).reshape(chan, entries).astype(bf16)
        value = value.reshape(groups * seqs, entries)
        high = value.astype(bf16)
        low = (value - high.astype(f32)).astype(bf16)
        dims = (((1,), (1,)), ((), ()))
        total = lax.dot_general(high, weight, dims, preferred_element_type=f32)
        return total + lax.dot_general(low, weight, dims, preferred_element_type=f32)

    read = read_out(new_re, out_re_ref) - read_out(new_im, out_im_ref)
    read = jnp.where(own_group, read.reshape(groups, seqs, chan), 0.0)
    read = jnp.sum(read, axis=0) + skip * drive.astype(f32)
    mixed = jax.nn.gelu(read).astype(bf16)
    mixed_ref[...] = mixed
    drain(state_re, new_sem.at[0])
    drain(state_im, new_sem.at[1])


def remote(src, dst, send, recv, axis, peer):
    copy = pltpu.make_async_remote_copy(
        src_ref=src,
        dst_ref=dst,
        send_sem=send,
        recv_sem=recv,
        device_id={axis: peer},
        device_id_type=MESH,
    )
    copy.start()


def drain(ref, sem):
    pltpu.make_async_copy(ref, ref, sem).wait()


def near_first(index, count):
    half = (index + 1) // 2
    odd = index % 2
    return half * odd + (count - half) * (1 - odd)


def exchange(
    n_tp,
    n_ep,
    mixed_ref,
    tokens_ref,
    bias_ref,
    gain_ref,
    route_ref,
    weight_ref,
    glu_hbm,
    out_w_hbm,
    gate_hbm,
    up_hbm,
    down_hbm,
    out_ref,
    glu_ref,
    out_w_ref,
    gate_w,
    up_w,
    down_w,
    ag_buf,
    rs_out,
    rs_in,
    disp,
    rows,
    xn,
    back_out,
    back_own,
    back_in,
    ret_out,
    ret_in,
    w_sem,
    ag_s,
    ag_r,
    rs_s,
    rs_r,
    disp_s,
    disp_r,
    fwd_s,
    fwd_r,
    back_s,
    back_r,
    ret_s,
    ret_r,
):
    tp = lax.axis_index("tp")
    ep = lax.axis_index("ep")
    seqs, chan = mixed_ref.shape
    width = out_ref.shape[1]
    blocks = rows.shape[2]
    slot_rows = blocks * 8
    slots = n_ep * slot_rows
    hidden_n = gate_w.shape[1]
    f32 = jnp.float32
    bf16 = jnp.bfloat16

    loads = [
        pltpu.make_async_copy(src, dst, w_sem.at[i])
        for i, (src, dst) in enumerate(
            (
                (glu_hbm, glu_ref),
                (out_w_hbm, out_w_ref),
                (gate_hbm.at[0], gate_w),
                (up_hbm.at[0], up_w),
                (down_hbm.at[0], down_w),
            )
        )
    ]
    for load in loads:
        load.start()

    barrier = pltpu.get_barrier_semaphore()

    @pl.loop(1, n_tp)
    def _(k):
        pl.semaphore_signal(
            barrier, inc=1, device_id={"tp": lax.rem(tp + k, n_tp)}, device_id_type=MESH
        )

    @pl.loop(1, n_ep)
    def _(k):
        pl.semaphore_signal(
            barrier, inc=1, device_id={"ep": lax.rem(ep + k, n_ep)}, device_id_type=MESH
        )

    pl.semaphore_wait(barrier, n_tp + n_ep - 2)

    def peer_at(k):
        return lax.rem(tp + k, n_tp)

    def source_at(k):
        return lax.rem(tp + n_tp - k, n_tp)

    for k in range(1, n_tp):
        remote(mixed_ref, ag_buf.at[k - 1], ag_s.at[k - 1], ag_r.at[k - 1], "tp", peer_at(k))

    def one_hot(index, size):
        return lax.broadcasted_iota(jnp.int32, (seqs, size), 1).astype(f32) == index

    row = lax.broadcasted_iota(jnp.int32, (seqs, seqs), 0)
    lane = lax.broadcasted_iota(jnp.int32, (seqs, seqs), 1)

    def upright(ref, k):
        value = ref[k : k + 1, :].astype(f32)
        return jnp.sum(jnp.where(row == lane, value, 0.0), axis=1, keepdims=True)

    choices = [upright(route_ref, k) for k in range(route_ref.shape[0])]
    hits = [one_hot(choice, n_ep).astype(f32) for choice in choices]
    earlier = jnp.where(lane < row, 1.0, 0.0).astype(bf16)
    before = jnp.dot(earlier, sum(hits).astype(bf16), preferred_element_type=f32)
    select = jnp.zeros((seqs, slots), f32)
    combine = jnp.zeros((seqs, slots), f32)
    for k, choice in enumerate(choices):
        rank = jnp.sum(before * hits[k], axis=1, keepdims=True)
        pick = one_hot(choice * slot_rows + rank, slots)
        select = jnp.where(pick, 1.0, select)
        combine = jnp.where(pick, upright(weight_ref, k), combine)

    mixed = mixed_ref[...]

    def glu_rows(owner):
        return glu_ref[pl.ds(pl.multiple_of(owner * chan, chan), chan), :]

    loads[0].wait()
    gate = jnp.dot(mixed, glu_rows(tp), preferred_element_type=f32) + bias_ref[...]
    for k in range(1, n_tp):
        drain(ag_buf.at[k - 1], ag_r.at[k - 1])
        gate += jnp.dot(ag_buf[k - 1], glu_rows(source_at(k)), preferred_element_type=f32)
    gated = (mixed.astype(f32) * jax.nn.sigmoid(gate)).astype(bf16)

    loads[1].wait()

    def columns(owner):
        return pl.ds(pl.multiple_of(owner * width, width), width)

    for k in range(1, n_tp):
        part = jnp.dot(gated, out_w_ref[:, columns(peer_at(k))], preferred_element_type=f32)
        rs_out[k - 1] = part.astype(bf16)
        remote(
            rs_out.at[k - 1], rs_in.at[k - 1], rs_s.at[k - 1], rs_r.at[k - 1], "tp", peer_at(k)
        )
    total = jnp.dot(gated, out_w_ref[:, columns(tp)], preferred_element_type=f32)
    total = total.astype(bf16).astype(f32)
    for k in range(1, n_tp):
        drain(rs_in.at[k - 1], rs_r.at[k - 1])
        total += rs_in[k - 1].astype(f32)
    resid = (tokens_ref[:, columns(tp)].astype(f32) + total).astype(bf16)

    picked = lax.dot_general(
        select.astype(bf16), resid, (((0,), (0,)), ((), ())), preferred_element_type=f32
    )
    disp[...] = picked.reshape(n_ep, blocks, 8, width).astype(bf16)

    @pl.loop(1, n_ep)
    def _(i):
        to = lax.rem(ep + near_first(i, n_ep), n_ep)
        remote(disp.at[to], rows.at[tp, i], disp_s, disp_r.at[i - 1], "ep", to)

    half = n_ep // 2
    for k in range(1, n_tp):
        remote(disp.at[ep], rows.at[tp, 0], fwd_s.at[k - 1], fwd_r.at[0, k - 1], "tp", peer_at(k))
    rows[tp, 0] = disp[ep]

    @pl.loop(1, n_ep)
    def _(i):
        here = rows.at[tp, i]
        drain(here, disp_r.at[i - 1])
        for k in range(1, n_tp):
            remote(here, here, fwd_s.at[k - 1], fwd_r.at[i // half, k - 1], "tp", peer_at(k))

    for part in range(2):
        span = pl.ds(part * half, half)

        def row_values(owner):
            return rows[owner, span].astype(f32).reshape(slots // 2, width)

        values = row_values(tp)
        squares = jnp.sum(values * values, axis=1, keepdims=True)
        for k in range(1, n_tp):
            drain(rows.at[source_at(k), span], fwd_r.at[part, k - 1])
            values = row_values(source_at(k))
            squares += jnp.sum(values * values, axis=1, keepdims=True)
        scale = lax.rsqrt(squares / (n_tp * width) + norm_eps)
        for owner in range(n_tp):
            cols = pl.ds(owner * width, width)
            xn[:, cols] = (row_values(owner) * scale * gain_ref[:, cols]).astype(bf16)

        if part == 0:
            loads[2].wait()
            loads[3].wait()
        pieces = []
        for start in range(0, hidden_n, 256):
            cols = pl.ds(start, min(256, hidden_n - start))
            gate_h = jnp.dot(xn[...], gate_w[:, cols], preferred_element_type=f32)
            up_h = jnp.dot(xn[...], up_w[:, cols], preferred_element_type=f32)
            pieces.append((jax.nn.silu(gate_h) * up_h).astype(bf16))
        hidden = jnp.concatenate(pieces, axis=1)
        if part == 0:
            loads[4].wait()

        def down(owner):
            value = jnp.dot(hidden, down_w[:, columns(owner)], preferred_element_type=f32)
            return value.reshape(half, blocks, 8, width).astype(bf16)

        for k in range(1, n_tp):
            back_out[k - 1, span] = down(peer_at(k))

            @pl.loop(part * half, part * half + half)
            def _(i):
                remote(
                    back_out.at[k - 1, i],
                    back_in.at[i, k - 1],
                    back_s.at[k - 1],
                    back_r.at[i],
                    "tp",
                    peer_at(k),
                )

        back_own[span] = down(tp)

    def settled(i):
        drain(back_in.at[i], back_r.at[i])
        result = back_own[i].astype(f32)
        for k in range(1, n_tp):
            result += back_in[i, k - 1].astype(f32)
        return result.astype(bf16)

    @pl.loop(1, n_ep)
    def _(i):
        to = lax.rem(ep + n_ep - near_first(i, n_ep), n_ep)
        ret_out[to] = settled(i)
        remote(ret_out.at[to], ret_in.at[ep], ret_s, ret_r.at[i - 1], "ep", to)

    ret_in[ep] = settled(0)

    @pl.loop(1, n_ep)
    def _(i):
        block = lax.rem(ep + near_first(i, n_ep), n_ep)
        drain(ret_in.at[block], ret_r.at[i - 1])

    returned = ret_in[...].astype(f32).reshape(slots, width).astype(bf16)
    high = combine.astype(bf16)
    low = (combine - high.astype(f32)).astype(bf16)
    expert_total = jnp.dot(high, returned, preferred_element_type=f32)
    expert_total += jnp.dot(low, returned, preferred_element_type=f32)
    out_ref[...] = (resid.astype(f32) + expert_total).astype(bf16)

    for k in range(1, n_tp):
        drain(mixed_ref, ag_s.at[k - 1])
        drain(rs_out.at[k - 1], rs_s.at[k - 1])
        drain(rows.at[0], fwd_s.at[k - 1])
        drain(back_out.at[k - 1], back_s.at[k - 1])
    drain(disp.at[pl.ds(0, n_ep - 1)], disp_s)
    drain(ret_out.at[pl.ds(0, n_ep - 1)], ret_s)


def local(
    tokens,
    mix_gain,
    w_in,
    decay_re,
    freq,
    log_step,
    in_re,
    in_im,
    out_re,
    out_im,
    skip,
    state_re,
    state_im,
    glu_weight,
    glu_bias,
    out_weight,
    ffn_gain,
    route,
    route_weight,
    expert_gate,
    expert_up,
    expert_down,
):
    seq_count, model_width = tokens.shape
    groups_local = decay_re.shape[0]
    n_tp = lax.axis_size("tp")
    experts = lax.axis_size("ep")
    local_width = model_width // n_tp
    top_count = route.shape[1]
    hidden_n = expert_gate.shape[2]
    slot_cap = (3 * seq_count * top_count + 2 * experts - 1) // (2 * experts)
    slot_rows = (slot_cap + 7) // 8 * 8
    slots = experts * slot_rows
    chan = w_in.shape[1]
    state_block = (groups_local, seq_count, state_re.shape[2])
    block = (slot_rows // 8, 8, local_width)
    bf16 = jnp.bfloat16
    dma = pltpu.SemaphoreType.DMA
    vmem = pl.BlockSpec(memory_space=pltpu.VMEM)
    anyplace = pl.BlockSpec(memory_space=pl.ANY)
    mixed_in, new_re, new_im = pl.pallas_call(
        state_kernel,
        out_shape=(
            jax.ShapeDtypeStruct((seq_count, chan), bf16),
            jax.ShapeDtypeStruct(state_re.shape, jnp.float32),
            jax.ShapeDtypeStruct(state_im.shape, jnp.float32),
        ),
        in_specs=[vmem] * 11 + [anyplace] * 2,
        out_specs=(vmem, anyplace, anyplace),
        scratch_shapes=[
            pltpu.VMEM(state_block, jnp.float32),
            pltpu.VMEM(state_block, jnp.float32),
            dma((2,)),
            dma((2,)),
        ],
    )(
        tokens,
        mix_gain[None, :],
        w_in,
        decay_re,
        freq,
        log_step[None, :],
        in_re,
        in_im,
        out_re,
        out_im,
        skip,
        state_re,
        state_im,
    )
    mixed = pl.pallas_call(
        functools.partial(exchange, n_tp, experts),
        out_shape=jax.ShapeDtypeStruct((seq_count, local_width), bf16),
        in_specs=[vmem] * 6 + [anyplace] * 5,
        out_specs=vmem,
        scratch_shapes=[
            pltpu.VMEM(glu_weight.shape, bf16),
            pltpu.VMEM(out_weight.shape, bf16),
            pltpu.VMEM((model_width, hidden_n), bf16),
            pltpu.VMEM((model_width, hidden_n), bf16),
            pltpu.VMEM((hidden_n, model_width), bf16),
            pltpu.VMEM((n_tp - 1, seq_count, chan), bf16),
            pltpu.VMEM((n_tp - 1, seq_count, local_width), bf16),
            pltpu.VMEM((n_tp - 1, seq_count, local_width), bf16),
            pltpu.VMEM((experts,) + block, bf16),
            pltpu.VMEM((n_tp, experts) + block, bf16),
            pltpu.VMEM((slots // 2, model_width), bf16),
            pltpu.VMEM((n_tp - 1, experts) + block, bf16),
            pltpu.VMEM((experts,) + block, bf16),
            pltpu.VMEM((experts, n_tp - 1) + block, bf16),
            pltpu.VMEM((experts,) + block, bf16),
            pltpu.VMEM((experts,) + block, bf16),
            dma((5,)),
            dma((n_tp - 1,)),
            dma((n_tp - 1,)),
            dma((n_tp - 1,)),
            dma((n_tp - 1,)),
            dma,
            dma((experts - 1,)),
            dma((n_tp - 1,)),
            dma((2, n_tp - 1)),
            dma((n_tp - 1,)),
            dma((experts,)),
            dma,
            dma((experts - 1,)),
        ],
        compiler_params=pltpu.CompilerParams(
            collective_id=0, has_side_effects=True, vmem_limit_bytes=61 * 1024 * 1024
        ),
    )(
        mixed_in,
        tokens,
        glu_bias[None, :],
        ffn_gain[None, :],
        route.T,
        route_weight.T,
        glu_weight,
        out_weight,
        expert_gate,
        expert_up,
        expert_down,
    )
    return (mixed, new_re, new_im)


def solution(mesh):
    in_specs = (
        P("ep", None),
        P(),
        P(None, "tp"),
        P("tp", None),
        P("tp", None),
        P("tp"),
        P("tp", None, None),
        P("tp", None, None),
        P("tp", None, None),
        P("tp", None, None),
        P("tp", None),
        P("ep", "tp", None),
        P("ep", "tp", None),
        P(None, "tp"),
        P("tp"),
        P("tp", None),
        P(),
        P("ep", None),
        P("ep", None),
        P("ep", None, "tp"),
        P("ep", None, "tp"),
        P("ep", "tp", None),
    )
    out_specs = (P("ep", "tp"), P("ep", "tp", None), P("ep", "tp", None))
    return jax.shard_map(local, mesh=mesh, in_specs=in_specs, out_specs=out_specs, check_vma=False)
```

profile of v0, /device:TPU:0, one launch (start us, length us, event | category | flops | bytes accessed | tf_op | source)
XLA Modules:
  0.0 46.8 jit_solution(2826391118187089932)
XLA Ops:
  0.6 4.6 %shard_map.229 = (bf16[64,256]{1,0:T(8,128)(2,1)}, f32[64,16,64]{2,1,0:T(8,128)}, f32[64,16,64]{2,1,0:T(8,128)}) custom-call(bf16[64,2048]{1,0:T(8,128)(2,1)} %tokens_ref.3, f32[1,2048]{1,0:T(1,128)} %bitcast.6, bf16[2048,256]{1,0:T(8,128)(2,1)} %w_in_ref.1, f32[16,64]{1,0:T(8,128)} %decay_ref.1, f32[16,64]{1,0:T(8,128)} %freq_ref.1, f32[1,16]{1,0:T(1,128)} %bitcast.11, ...), custom_call_target="tpu_custom_call" | custom-call | tf_op jit(solution)/shard_map/pallas_call | solution.py:443
  5.3 40.1 %shard_map.230 = bf16[64,512]{1,0:T(8,128)(2,1)} custom-call(bf16[64,256]{1,0:T(8,128)(2,1)} %get-tuple-element.6.mixed_ref, bf16[64,2048]{1,0:T(8,128)(2,1)} %tokens_ref.3, f32[1,256]{1,0:T(1,128)} %bitcast.8, f32[1,2048]{1,0:T(1,128)} %bitcast.7, s32[2,64]{1,0:T(2,128)} %bitcast.9, f32[2,64]{1,0:T(2,128)} %bitcast.10, bf16[1024,256]{1,0:T(8,128)(2,1)} %glu_hbm.1, ...), custom_call_target="tpu_custom_call" | custom-call | tf_op jit(solution)/shard_map/pallas_call | solution.py:473
  45.3 1.5 %copy.26 = bf16[64,512]{1,0:T(8,128)(2,1)} copy(bf16[64,512]{1,0:T(8,128)(2,1)} %shard_map.230) | data formatting | bytes 131072
where the time goes:
time: 47.1 us; the launch traced here: 46.8 us
  Pallas kernels  44.7 us (95%)
  local copies, waits for them, and re-layouts  1.47 us (3%)
  between operations  0.65 us (1%)
    pallas_call x1, Pallas kernels, local(): pl.pallas_call(functools.partial(exchange, n_tp, experts), out_shape=jax....  40.1 us
    pallas_call x1, Pallas kernels, local(): pl.pallas_call(state_kernel, out_shape=(jax.ShapeDtypeStruct((seq_count,...  4.61 us
    unnamed x1, local copies, waits for them, and re-layouts  1.47 us

commit v1 on v0

v1 whole, which is shorter than its diff:
```python
import functools
import jax
import jax.numpy as jnp
from jax import lax
from jax.experimental import pallas as pl
from jax.experimental.pallas import tpu as pltpu
from jax.sharding import PartitionSpec as P

norm_eps = 1e-06
MESH = pl.DeviceIdType.MESH


def rms_scale(rows, gain):
    values = rows.astype(jnp.float32)
    scaled = values * lax.rsqrt(jnp.mean(values * values, axis=-1, keepdims=True) + norm_eps)
    return (scaled * gain).astype(jnp.bfloat16)


def drain(ref, sem):
    pltpu.make_async_copy(ref, ref, sem).wait()


def remote(src, dst, send, recv, axis, peer):
    copy = pltpu.make_async_remote_copy(
        src_ref=src,
        dst_ref=dst,
        send_sem=send,
        recv_sem=recv,
        device_id={axis: peer},
        device_id_type=MESH,
    )
    copy.start()


def paired(index, offset, count):
    result, bit = 0, 1
    while bit < count:
        result += lax.rem(lax.div(index, bit) + lax.div(offset, bit), 2) * bit
        bit *= 2
    return result


def each(low, high, body):
    if high - low <= 8:
        for i in range(low, high):
            body(i)
    else:
        pl.loop(low, high)(body)


def chunks_of(n_ep):
    half, quarter = n_ep // 2, n_ep // 4
    return ((0, half), (half, quarter), (half + quarter, n_ep - half - quarter))


SMALL = (
    "tokens",
    "mix_gain",
    "decay",
    "freq",
    "log_step",
    "in_re",
    "in_im",
    "w_in",
    "out_re",
    "out_im",
    "skip",
)
LATER = ("glu", "bias", "route", "weight", "out_w", "gain", "gate", "up", "down")


def mixer(v, wait, state_re, state_im, state_sem):
    f32 = jnp.float32
    bf16 = jnp.bfloat16
    groups, places, entries = v["in_re"].shape
    seqs = v["tokens"].shape[0]
    chan = v["w_in"].shape[1]

    for name in ("decay", "freq", "log_step"):
        wait(name)
    diagonal = lax.broadcasted_iota(jnp.int32, (groups, groups), 0)
    diagonal = diagonal == lax.broadcasted_iota(jnp.int32, (groups, groups), 1)
    log_step = jnp.sum(jnp.where(diagonal, v["log_step"][...], 0.0), axis=1, keepdims=True)
    step = jnp.exp(log_step)
    decay = v["decay"][...]
    freq = v["freq"][...]
    magnitude = jnp.exp(decay * step)
    turn_re = magnitude * jnp.cos(freq * step)
    turn_im = magnitude * jnp.sin(freq * step)
    denom = decay * decay + freq * freq
    coef_re = ((turn_re - 1.0) * decay + turn_im * freq) / denom
    coef_im = (turn_im * decay - (turn_re - 1.0) * freq) / denom

    def lane_group(shape):
        lane = lax.broadcasted_iota(jnp.int32, shape, len(shape) - 1)
        first = lax.broadcasted_iota(jnp.int32, shape, 0) * places
        return (lane >= first) & (lane < first + places)

    wait("tokens")
    wait("mix_gain")
    normed = rms_scale(v["tokens"][...], v["mix_gain"][...])
    wait("w_in")
    drive = jnp.dot(normed, v["w_in"][...], preferred_element_type=f32).astype(bf16)
    own_group = lane_group((groups, seqs, chan))
    apart = jnp.where(own_group, drive.astype(f32)[None], 0.0).astype(bf16)
    apart = apart.reshape(groups * seqs, chan)

    def driven(ref):
        weight = ref[...].astype(f32).reshape(chan, entries).astype(bf16)
        value = jnp.dot(apart, weight, preferred_element_type=f32)
        return value.reshape(groups, seqs, entries)

    for name in ("in_re", "in_im"):
        wait(name)
    drive_re, drive_im = driven(v["in_re"]), driven(v["in_im"])
    turn_re, turn_im = turn_re[:, None, :], turn_im[:, None, :]
    coef_re, coef_im = coef_re[:, None, :], coef_im[:, None, :]
    drain(state_re, state_sem.at[0])
    drain(state_im, state_sem.at[1])
    old_re, old_im = state_re[...], state_im[...]
    new_re = turn_re * old_re - turn_im * old_im + (coef_re * drive_re - coef_im * drive_im)
    new_im = turn_re * old_im + turn_im * old_re + (coef_re * drive_im + coef_im * drive_re)
    state_re[...] = new_re
    state_im[...] = new_im

    def read_out(value, ref):
        weight = ref[...].astype(f32).reshape(chan, entries).astype(bf16)
        value = value.reshape(groups * seqs, entries)
        high = value.astype(bf16)
        low = (value - high.astype(f32)).astype(bf16)
        dims = (((1,), (1,)), ((), ()))
        total = lax.dot_general(high, weight, dims, preferred_element_type=f32)
        return total + lax.dot_general(low, weight, dims, preferred_element_type=f32)

    for name in ("out_re", "out_im", "skip"):
        wait(name)
    spread = lax.broadcasted_iota(jnp.int32, (places, chan), 1) % places
    spread = spread == lax.broadcasted_iota(jnp.int32, (places, chan), 0)
    skip = jnp.dot(
        v["skip"][...],
        spread.astype(f32),
        precision=lax.Precision.HIGHEST,
        preferred_element_type=f32,
    )
    skip = jnp.sum(jnp.where(lane_group((groups, chan)), skip, 0.0), axis=0, keepdims=True)
    read = read_out(new_re, v["out_re"]) - read_out(new_im, v["out_im"])
    read = jnp.where(own_group, read.reshape(groups, seqs, chan), 0.0)
    read = jnp.sum(read, axis=0) + skip * drive.astype(f32)
    return jax.nn.gelu(read).astype(bf16)


def layer(n_tp, n_ep, *refs):
    f32 = jnp.float32
    bf16 = jnp.bfloat16
    names = SMALL + LATER
    hbm = dict(zip(names, refs))
    state_re_hbm, state_im_hbm, out_ref, state_re, state_im = refs[len(names) : len(names) + 5]
    rest = refs[len(names) + 5 :]
    v = dict(zip(names, rest))
    (
        mixed_ref,
        ag_buf,
        rs_out,
        rs_in,
        disp,
        rows,
        xn,
        back_out,
        back_own,
        back_in,
        ret_out,
        ret_in,
        load_sem,
        state_sem,
        ag_s,
        ag_r,
        rs_s,
        rs_r,
        disp_s,
        disp_r,
        fwd_s,
        fwd_r,
        back_s,
        back_r,
        ret_s,
        ret_r,
    ) = rest[len(names) :]
    tp = lax.axis_index("tp")
    ep = lax.axis_index("ep")
    seqs, chan = mixed_ref.shape
    width = out_ref.shape[1]
    blocks = rows.shape[2]
    slot_rows = blocks * 8
    slots = n_ep * slot_rows
    hidden_n = v["gate"].shape[1]
    peers = tuple(range(n_tp - 1, 0, -1))
    chunks = chunks_of(n_ep)

    def copy_of(name):
        src = hbm[name]
        if name in ("gate", "up", "down"):
            src = src.at[0]
        return pltpu.make_async_copy(src, v[name], load_sem.at[names.index(name)])

    def wait(name):
        copy_of(name).wait()

    for name in SMALL:
        copy_of(name).start()

    @pl.loop(0, state_re.shape[0])
    def _(g):
        for i, (far, near) in enumerate(((state_re_hbm, state_re), (state_im_hbm, state_im))):
            pltpu.make_async_copy(far.at[:, g, :], near.at[g], state_sem.at[i]).start()

    for name in LATER:
        copy_of(name).start()

    barrier = pltpu.get_barrier_semaphore()

    @pl.loop(1, n_tp)
    def _(k):
        pl.semaphore_signal(
            barrier, inc=1, device_id={"tp": lax.rem(tp + k, n_tp)}, device_id_type=MESH
        )

    @pl.loop(1, n_ep)
    def _(k):
        pl.semaphore_signal(
            barrier, inc=1, device_id={"ep": lax.rem(ep + k, n_ep)}, device_id_type=MESH
        )

    def tp_peer(k):
        return paired(tp, k, n_tp)

    def ep_peer(i):
        return paired(ep, i, n_ep)

    mixed = mixer(v, wait, state_re, state_im, state_sem)
    mixed_ref[...] = mixed
    pl.semaphore_wait(barrier, n_tp + n_ep - 2)
    for k in peers:
        remote(mixed_ref, ag_buf.at[k - 1], ag_s.at[k - 1], ag_r.at[k - 1], "tp", tp_peer(k))

    def one_hot(index, size):
        return lax.broadcasted_iota(jnp.int32, (seqs, size), 1).astype(f32) == index

    row = lax.broadcasted_iota(jnp.int32, (seqs, seqs), 0)
    lane = lax.broadcasted_iota(jnp.int32, (seqs, seqs), 1)

    def upright(ref, k):
        value = ref[k : k + 1, :].astype(f32)
        return jnp.sum(jnp.where(row == lane, value, 0.0), axis=1, keepdims=True)

    for name in ("route", "weight", "bias", "gain"):
        wait(name)
    route_ref, weight_ref, gain_ref = v["route"], v["weight"], v["gain"]
    choices = [upright(route_ref, k) for k in range(route_ref.shape[0])]
    hits = [one_hot(choice, n_ep).astype(f32) for choice in choices]
    earlier = jnp.where(lane < row, 1.0, 0.0).astype(bf16)
    before = jnp.dot(earlier, sum(hits).astype(bf16), preferred_element_type=f32)
    select = jnp.zeros((seqs, slots), f32)
    combine = jnp.zeros((seqs, slots), f32)
    for k, choice in enumerate(choices):
        rank = jnp.sum(before * hits[k], axis=1, keepdims=True)
        pick = one_hot(choice * slot_rows + rank, slots)
        select = jnp.where(pick, 1.0, select)
        combine = jnp.where(pick, upright(weight_ref, k), combine)

    def glu_rows(owner):
        return v["glu"][pl.ds(pl.multiple_of(owner * chan, chan), chan), :]

    wait("glu")
    gate = jnp.dot(mixed, glu_rows(tp), preferred_element_type=f32) + v["bias"][...]
    for k in reversed(peers):
        drain(ag_buf.at[k - 1], ag_r.at[k - 1])
        gate += jnp.dot(ag_buf[k - 1], glu_rows(tp_peer(k)), preferred_element_type=f32)
    gated = (mixed.astype(f32) * jax.nn.sigmoid(gate)).astype(bf16)

    wait("out_w")

    def columns(owner):
        return pl.ds(pl.multiple_of(owner * width, width), width)

    for k in peers:
        part = jnp.dot(gated, v["out_w"][:, columns(tp_peer(k))], preferred_element_type=f32)
        rs_out[k - 1] = part.astype(bf16)
        remote(
            rs_out.at[k - 1], rs_in.at[k - 1], rs_s.at[k - 1], rs_r.at[k - 1], "tp", tp_peer(k)
        )
    total = jnp.dot(gated, v["out_w"][:, columns(tp)], preferred_element_type=f32)
    total = total.astype(bf16).astype(f32)
    for k in reversed(peers):
        drain(rs_in.at[k - 1], rs_r.at[k - 1])
        total += rs_in[k - 1].astype(f32)
    resid = (v["tokens"][:, columns(tp)].astype(f32) + total).astype(bf16)

    picked = lax.dot_general(
        select.astype(bf16), resid, (((0,), (0,)), ((), ())), preferred_element_type=f32
    )
    disp[...] = picked.reshape(n_ep, blocks, 8, width).astype(bf16)

    def dispatch(i):
        to = ep_peer(i)
        remote(disp.at[to], rows.at[tp, i], disp_s, disp_r.at[i - 1], "ep", to)

    each(1, n_ep, dispatch)

    for k in peers:
        remote(disp.at[ep], rows.at[tp, 0], fwd_s.at[k - 1], fwd_r.at[0, k - 1], "tp", tp_peer(k))
    rows[tp, 0] = disp[ep]

    for part, (start, count) in enumerate(chunks):

        def forward(i, part=part):
            here = rows.at[tp, i]
            drain(here, disp_r.at[i - 1])
            for k in peers:
                remote(here, here, fwd_s.at[k - 1], fwd_r.at[part, k - 1], "tp", tp_peer(k))

        each(max(start, 1), start + count, forward)

    for part, (start, count) in enumerate(chunks):
        span = pl.ds(start, count)
        held = xn.at[pl.ds(0, count * slot_rows)]

        def row_values(owner):
            return rows[owner, span].astype(f32).reshape(count * slot_rows, width)

        values = row_values(tp)
        squares = jnp.sum(values * values, axis=1, keepdims=True)
        for k in reversed(peers):
            drain(rows.at[tp_peer(k), span], fwd_r.at[part, k - 1])
            values = row_values(tp_peer(k))
            squares += jnp.sum(values * values, axis=1, keepdims=True)
        scale = lax.rsqrt(squares / (n_tp * width) + norm_eps)
        for owner in range(n_tp):
            cols = pl.ds(owner * width, width)
            held[:, cols] = (row_values(owner) * scale * gain_ref[:, cols]).astype(bf16)

        if part == 0:
            wait("gate")
            wait("up")
        pieces = []
        for first in range(0, hidden_n, 256):
            cols = pl.ds(first, min(256, hidden_n - first))
            gate_h = jnp.dot(held[...], v["gate"][:, cols], preferred_element_type=f32)
            up_h = jnp.dot(held[...], v["up"][:, cols], preferred_element_type=f32)
            pieces.append((jax.nn.silu(gate_h) * up_h).astype(bf16))
        hidden = jnp.concatenate(pieces, axis=1)
        if part == 0:
            wait("down")

        def down(owner):
            value = jnp.dot(hidden, v["down"][:, columns(owner)], preferred_element_type=f32)
            return value.reshape(count, blocks, 8, width).astype(bf16)

        for k in peers:
            back_out[k - 1, span] = down(tp_peer(k))
            remote(
                back_out.at[k - 1, span],
                back_in.at[k - 1, span],
                back_s.at[k - 1],
                back_r.at[part, k - 1],
                "tp",
                tp_peer(k),
            )
        back_own[span] = down(tp)

    for part, (start, count) in enumerate(chunks):
        for k in peers:
            drain(back_in.at[k - 1, pl.ds(start, count)], back_r.at[part, k - 1])

        def settle(i):
            result = back_own[i].astype(f32)
            for k in reversed(peers):
                result += back_in[k - 1, i].astype(f32)
            result = result.astype(bf16)
            if isinstance(i, int) and i == 0:
                ret_in[ep] = result
                return
            to = ep_peer(i)
            ret_out[to] = result
            remote(ret_out.at[to], ret_in.at[ep], ret_s, ret_r.at[i - 1], "ep", to)

        if start == 0:
            settle(0)
        each(max(start, 1), start + count, settle)

    def arrived(i):
        drain(ret_in.at[ep_peer(i)], ret_r.at[i - 1])

    each(1, n_ep, arrived)

    returned = ret_in[...].astype(f32).reshape(slots, width).astype(bf16)
    high = combine.astype(bf16)
    low = (combine - high.astype(f32)).astype(bf16)
    expert_total = jnp.dot(high, returned, preferred_element_type=f32)
    expert_total += jnp.dot(low, returned, preferred_element_type=f32)
    out_ref[...] = (resid.astype(f32) + expert_total).astype(bf16)

    for k in peers:
        drain(mixed_ref, ag_s.at[k - 1])
        drain(rs_out.at[k - 1], rs_s.at[k - 1])
        drain(rows.at[0], fwd_s.at[k - 1])
        drain(back_out.at[k - 1], back_s.at[k - 1])
    drain(disp.at[pl.ds(0, n_ep - 1)], disp_s)
    drain(ret_out.at[pl.ds(0, n_ep - 1)], ret_s)


def store(mixed_ref, re_ref, im_ref, mixed_hbm, re_hbm, im_hbm, sem):
    out = pltpu.make_async_copy(mixed_ref, mixed_hbm, sem.at[0])
    out.start()

    @pl.loop(0, re_ref.shape[0])
    def _(g):
        for i, (near, far) in enumerate(((re_ref, re_hbm), (im_ref, im_hbm))):
            pltpu.make_async_copy(near.at[g], far.at[:, g, :], sem.at[i + 1]).start()

    out.wait()
    drain(re_ref, sem.at[1])
    drain(im_ref, sem.at[2])


def local(
    tokens,
    mix_gain,
    w_in,
    decay_re,
    freq,
    log_step,
    in_re,
    in_im,
    out_re,
    out_im,
    skip,
    state_re,
    state_im,
    glu_weight,
    glu_bias,
    out_weight,
    ffn_gain,
    route,
    route_weight,
    expert_gate,
    expert_up,
    expert_down,
):
    seq_count, model_width = tokens.shape
    n_tp = lax.axis_size("tp")
    experts = lax.axis_size("ep")
    local_width = model_width // n_tp
    top_count = route.shape[1]
    slot_cap = (3 * seq_count * top_count + 2 * experts - 1) // (2 * experts)
    slot_rows = (slot_cap + 7) // 8 * 8
    chan = w_in.shape[1]
    state_block = (decay_re.shape[0], seq_count, state_re.shape[2])
    block = (slot_rows // 8, 8, local_width)
    chunks = chunks_of(experts)
    bf16 = jnp.bfloat16
    dma = pltpu.SemaphoreType.DMA
    vmem = pl.BlockSpec(memory_space=pltpu.VMEM)
    anyplace = pl.BlockSpec(memory_space=pl.ANY)
    arrays = {
        "tokens": tokens,
        "mix_gain": mix_gain[None, :],
        "w_in": w_in,
        "decay": decay_re,
        "freq": freq,
        "log_step": log_step[None, :],
        "in_re": in_re,
        "in_im": in_im,
        "out_re": out_re,
        "out_im": out_im,
        "skip": skip,
        "glu": glu_weight,
        "bias": glu_bias[None, :],
        "out_w": out_weight,
        "gain": ffn_gain[None, :],
        "route": route.T,
        "weight": route_weight.T,
        "gate": expert_gate,
        "up": expert_up,
        "down": expert_down,
    }
    arrays = [arrays[name] for name in SMALL + LATER]
    holds = [
        pltpu.VMEM(a.shape[1:] if name in ("gate", "up", "down") else a.shape, a.dtype)
        for name, a in zip(SMALL + LATER, arrays)
    ]
    mixed, new_re, new_im = pl.pallas_call(
        functools.partial(layer, n_tp, experts),
        out_shape=(
            pltpu.VMEM((seq_count, local_width), bf16),
            pltpu.VMEM(state_block, jnp.float32),
            pltpu.VMEM(state_block, jnp.float32),
        ),
        in_specs=[anyplace] * (len(arrays) + 2),
        out_specs=(vmem, vmem, vmem),
        scratch_shapes=holds
        + [
            pltpu.VMEM((seq_count, chan), bf16),
            pltpu.VMEM((n_tp - 1, seq_count, chan), bf16),
            pltpu.VMEM((n_tp - 1, seq_count, local_width), bf16),
            pltpu.VMEM((n_tp - 1, seq_count, local_width), bf16),
            pltpu.VMEM((experts,) + block, bf16),
            pltpu.VMEM((n_tp, experts) + block, bf16),
            pltpu.VMEM((max(c for _, c in chunks) * slot_rows, model_width), bf16),
            pltpu.VMEM((n_tp - 1, experts) + block, bf16),
            pltpu.VMEM((experts,) + block, bf16),
            pltpu.VMEM((n_tp - 1, experts) + block, bf16),
            pltpu.VMEM((experts,) + block, bf16),
            pltpu.VMEM((experts,) + block, bf16),
            dma((len(arrays),)),
            dma((2,)),
            dma((n_tp - 1,)),
            dma((n_tp - 1,)),
            dma((n_tp - 1,)),
            dma((n_tp - 1,)),
            dma,
            dma((experts - 1,)),
            dma((n_tp - 1,)),
            dma((len(chunks), n_tp - 1)),
            dma((n_tp - 1,)),
            dma((len(chunks), n_tp - 1)),
            dma,
            dma((experts - 1,)),
        ],
        compiler_params=pltpu.CompilerParams(
            collective_id=0, has_side_effects=True, vmem_limit_bytes=58 * 1024 * 1024
        ),
    )(*arrays, state_re, state_im)
    results = [pltpu.with_memory_space_constraint(a, pltpu.VMEM) for a in (mixed, new_re, new_im)]
    return pl.pallas_call(
        store,
        out_shape=(
            jax.ShapeDtypeStruct((seq_count, local_width), bf16),
            jax.ShapeDtypeStruct(state_re.shape, jnp.float32),
            jax.ShapeDtypeStruct(state_im.shape, jnp.float32),
        ),
        in_specs=[vmem] * 3,
        out_specs=(anyplace,) * 3,
        scratch_shapes=[dma((3,))],
    )(*results)


def solution(mesh):
    in_specs = (
        P("ep", None),
        P(),
        P(None, "tp"),
        P("tp", None),
        P("tp", None),
        P("tp"),
        P("tp", None, None),
        P("tp", None, None),
        P("tp", None, None),
        P("tp", None, None),
        P("tp", None),
        P("ep", "tp", None),
        P("ep", "tp", None),
        P(None, "tp"),
        P("tp"),
        P("tp", None),
        P(),
        P("ep", None),
        P("ep", None),
        P("ep", None, "tp"),
        P("ep", None, "tp"),
        P("ep", "tp", None),
    )
    out_specs = (P("ep", "tp"), P("ep", "tp", None), P("ep", "tp", None))
    return jax.shard_map(local, mesh=mesh, in_specs=in_specs, out_specs=out_specs, check_vma=False)
```

time: 47.1 us -> 41.6 us (0.88)
  Pallas kernels: 44.7 us -> 40.8 us
  local copies, waits for them, and re-layouts: 1.47 us -> 0 us
    pallas_call x2, Pallas kernels: 44.7 us -> 40.8 us  [the longest x1 39.8 us: local(): pl.pallas_call(functools.partial(layer, n_tp, experts), out_shape=(pltpu....]
    unnamed x1 -> x0, local copies, waits for them, and re-layouts: 1.47 us -> none
where the time goes in v1:
time: 41.6 us; the launch traced here: 41.5 us
  Pallas kernels  40.8 us (98%)
  between operations  0.65 us (2%)
    pallas_call x1, Pallas kernels, local(): pl.pallas_call(functools.partial(layer, n_tp, experts), out_shape=(pltpu....  39.8 us
    pallas_call x1, Pallas kernels, local(): pl.pallas_call(store, out_shape=(jax.ShapeDtypeStruct((seq_count, local_w...  0.99 us

profile of v1, /device:TPU:0, one launch (start us, length us, event | category | flops | bytes accessed | tf_op | source)
XLA Modules:
  0.0 41.5 jit_solution(5778387817370232826)
XLA Ops:
  0.6 39.8 %shard_map.229 = (bf16[64,512]{1,0:T(8,128)(2,1)S(1)}, f32[16,64,64]{2,1,0:T(8,128)S(1)}, f32[16,64,64]{2,1,0:T(8,128)S(1)}) custom-call(bf16[64,2048]{1,0:T(8,128)(2,1)} %refs_0_.1, f32[1,2048]{1,0:T(1,128)} %bitcast.6, f32[16,64]{1,0:T(8,128)} %refs_2_.1, f32[16,64]{1,0:T(8,128)} %refs_3_.1, f32[1,16]{1,0:T(1,128)} %bitcast.11, ...), custom_call_target="tpu_custom_call" | custom-call | tf_op jit(solution)/shard_map/pallas_call | solution.py:491
  40.5 1.0 %shard_map.230 = (bf16[64,512]{1,0:T(8,128)(2,1)}, f32[64,16,64]{2,1,0:T(8,128)}, f32[64,16,64]{2,1,0:T(8,128)}) custom-call(bf16[64,512]{1,0:T(8,128)(2,1)S(1)} %get-tuple-element.6.mixed_ref, f32[16,64,64]{2,1,0:T(8,128)S(1)} %get-tuple-element.7.re_ref, f32[16,64,64]{2,1,0:T(8,128)S(1)} %get-tuple-element.8.im_ref), custom_call_target="tpu_custom_call" | custom-call | tf_op jit(solution)/shard_map/pallas_call | solution.py:534

commit v2 on v1

--- a/solution.py
+++ b/solution.py
@@ -38,6 +38,11 @@
         result += lax.rem(lax.div(index, bit) + lax.div(offset, bit), 2) * bit
         bit *= 2
     return result
+
+
+def offset_at(place, count):
+    pair, core = place // 2 * 2, place % 2
+    return (count - pair) % count + core
 
 
 def each(low, high, body):
@@ -147,6 +152,10 @@
     read = jnp.where(own_group, read.reshape(groups, seqs, chan), 0.0)
     read = jnp.sum(read, axis=0) + skip * drive.astype(f32)
     return jax.nn.gelu(read).astype(bf16)
+
+
+def gated_unit(gate, up):
+    return (jax.nn.silu(gate) * up).astype(jnp.bfloat16)
 
 
 def layer(n_tp, n_ep, *refs):
@@ -195,6 +204,7 @@
     hidden_n = v["gate"].shape[1]
     peers = tuple(range(n_tp - 1, 0, -1))
     chunks = chunks_of(n_ep)
+    first_part = [start for start, _ in chunks].index(0)
 
     def copy_of(name):
         src = hbm[name]
@@ -234,7 +244,7 @@
         return paired(tp, k, n_tp)
 
     def ep_peer(i):
-        return paired(ep, i, n_ep)
+        return paired(ep, offset_at(i, n_ep), n_ep)
 
     mixed = mixer(v, wait, state_re, state_im, state_sem)
     mixed_ref[...] = mixed
@@ -282,14 +292,17 @@
     def columns(owner):
         return pl.ds(pl.multiple_of(owner * width, width), width)
 
-    for k in peers:
-        part = jnp.dot(gated, v["out_w"][:, columns(tp_peer(k))], preferred_element_type=f32)
-        rs_out[k - 1] = part.astype(bf16)
+    def share(owner):
+        value = jnp.dot(gated, v["out_w"][:, columns(owner)], preferred_element_type=f32)
+        return value.astype(bf16)
+
+    shares = [share(tp_peer(k)) for k in peers] if n_tp <= 4 else None
+    for at, k in enumerate(peers):
+        rs_out[k - 1] = shares[at] if shares else share(tp_peer(k))
         remote(
             rs_out.at[k - 1], rs_in.at[k - 1], rs_s.at[k - 1], rs_r.at[k - 1], "tp", tp_peer(k)
         )
-    total = jnp.dot(gated, v["out_w"][:, columns(tp)], preferred_element_type=f32)
-    total = total.astype(bf16).astype(f32)
+    total = share(tp).astype(f32)
     for k in reversed(peers):
         drain(rs_in.at[k - 1], rs_r.at[k - 1])
         total += rs_in[k - 1].astype(f32)
@@ -307,10 +320,10 @@
     each(1, n_ep, dispatch)
 
     for k in peers:
-        remote(disp.at[ep], rows.at[tp, 0], fwd_s.at[k - 1], fwd_r.at[0, k - 1], "tp", tp_peer(k))
+        remote(disp.at[ep], rows.at[tp, 0], fwd_s.at[k - 1], fwd_r.at[first_part, k - 1], "tp", tp_peer(k))
     rows[tp, 0] = disp[ep]
 
-    for part, (start, count) in enumerate(chunks):
+    for start, part, count in sorted((start, part, count) for part, (start, count) in enumerate(chunks)):
 
         def forward(i, part=part):
             here = rows.at[tp, i]
@@ -327,12 +340,10 @@
         def row_values(owner):
             return rows[owner, span].astype(f32).reshape(count * slot_rows, width)
 
-        values = row_values(tp)
-        squares = jnp.sum(values * values, axis=1, keepdims=True)
         for k in reversed(peers):
             drain(rows.at[tp_peer(k), span], fwd_r.at[part, k - 1])
-            values = row_values(tp_peer(k))
-            squares += jnp.sum(values * values, axis=1, keepdims=True)
+        squares = sum(row_values(owner) * row_values(owner) for owner in range(n_tp))
+        squares = jnp.sum(squares, axis=1, keepdims=True)
         scale = lax.rsqrt(squares / (n_tp * width) + norm_eps)
         for owner in range(n_tp):
             cols = pl.ds(owner * width, width)
@@ -341,13 +352,10 @@
         if part == 0:
             wait("gate")
             wait("up")
-        pieces = []
-        for first in range(0, hidden_n, 256):
-            cols = pl.ds(first, min(256, hidden_n - first))
-            gate_h = jnp.dot(held[...], v["gate"][:, cols], preferred_element_type=f32)
-            up_h = jnp.dot(held[...], v["up"][:, cols], preferred_element_type=f32)
-            pieces.append((jax.nn.silu(gate_h) * up_h).astype(bf16))
-        hidden = jnp.concatenate(pieces, axis=1)
+        products = (
+            jnp.dot(held[...], v[name][...], preferred_element_type=f32) for name in ("gate", "up")
+        )
+        hidden = gated_unit(*products)
         if part == 0:
             wait("down")
 
@@ -355,8 +363,8 @@
             value = jnp.dot(hidden, v["down"][:, columns(owner)], preferred_element_type=f32)
             return value.reshape(count, blocks, 8, width).astype(bf16)
 
-        for k in peers:
-            back_out[k - 1, span] = down(tp_peer(k))
+        def give_back(k, value):
+            back_out[k - 1, span] = value
             remote(
                 back_out.at[k - 1, span],
                 back_in.at[k - 1, span],
@@ -365,7 +373,16 @@
                 "tp",
                 tp_peer(k),
             )
-        back_own[span] = down(tp)
+
+        ready = None
+        for k in peers:
+            value = down(tp_peer(k))
+            if ready is not None:
+                give_back(*ready)
+            ready = k, value
+        own = down(tp)
+        give_back(*ready)
+        back_own[span] = own
 
     for part, (start, count) in enumerate(chunks):
         for k in peers:

time: 41.6 us -> 40 us (0.962)
  Pallas kernels: 40.8 us -> 39.2 us
    pallas_call x1, Pallas kernels: 39.8 us -> 38.2 us  [local(): pl.pallas_call(functools.partial(layer, n_tp, experts), out_shape=(pltpu....]
where the time goes in v2:
time: 40 us; the launch traced here: 39.8 us
  Pallas kernels  39.2 us (98%)
  between operations  0.65 us (2%)
    pallas_call x1, Pallas kernels, local(): pl.pallas_call(functools.partial(layer, n_tp, experts), out_shape=(pltpu....  38.2 us
    pallas_call x1, Pallas kernels, local(): pl.pallas_call(store, out_shape=(jax.ShapeDtypeStruct((seq_count, local_w...  0.99 us

profile of v2, /device:TPU:0, one launch (start us, length us, event | category | flops | bytes accessed | tf_op | source)
XLA Modules:
  0.0 39.8 jit_solution(16969356748211862889)
XLA Ops:
  0.6 38.2 %shard_map.229 = (bf16[64,512]{1,0:T(8,128)(2,1)S(1)}, f32[16,64,64]{2,1,0:T(8,128)S(1)}, f32[16,64,64]{2,1,0:T(8,128)S(1)}) custom-call(bf16[64,2048]{1,0:T(8,128)(2,1)} %refs_0_.1, f32[1,2048]{1,0:T(1,128)} %bitcast.6, f32[16,64]{1,0:T(8,128)} %refs_2_.1, f32[16,64]{1,0:T(8,128)} %refs_3_.1, f32[1,16]{1,0:T(1,128)} %bitcast.11, ...), custom_call_target="tpu_custom_call" | custom-call | tf_op jit(solution)/shard_map/pallas_call | solution.py:508
  38.8 1.0 %shard_map.230 = (bf16[64,512]{1,0:T(8,128)(2,1)}, f32[64,16,64]{2,1,0:T(8,128)}, f32[64,16,64]{2,1,0:T(8,128)}) custom-call(bf16[64,512]{1,0:T(8,128)(2,1)S(1)} %get-tuple-element.6.mixed_ref, f32[16,64,64]{2,1,0:T(8,128)S(1)} %get-tuple-element.7.re_ref, f32[16,64,64]{2,1,0:T(8,128)S(1)} %get-tuple-element.8.im_ref), custom_call_target="tpu_custom_call" | custom-call | tf_op jit(solution)/shard_map/pallas_call | solution.py:551

commit v3 on v2

--- a/solution.py
+++ b/solution.py
@@ -41,8 +41,8 @@
 
 
 def offset_at(place, count):
-    pair, core = place // 2 * 2, place % 2
-    return (count - pair) % count + core
+    core = place % 2
+    return count - 2 - (place - core) + core
 
 
 def each(low, high, body):
@@ -53,20 +53,23 @@
         pl.loop(low, high)(body)
 
 
-def chunks_of(n_ep):
-    half, quarter = n_ep // 2, n_ep // 4
-    return ((0, half), (half, quarter), (half + quarter, n_ep - half - quarter))
+def groups_of(n_ep):
+    quarter = n_ep // 4
+    return tuple((part * quarter, quarter) for part in range(4))
+
+
+PASSES = ((0,), (1,), (2, 3))
 
 
 SMALL = (
     "tokens",
+    "w_in",
     "mix_gain",
     "decay",
     "freq",
     "log_step",
     "in_re",
     "in_im",
-    "w_in",
     "out_re",
     "out_im",
     "skip",
@@ -80,12 +83,33 @@
     groups, places, entries = v["in_re"].shape
     seqs = v["tokens"].shape[0]
     chan = v["w_in"].shape[1]
-
-    for name in ("decay", "freq", "log_step"):
+    wide = groups * entries
+
+    def spread(value):
+        pair = jnp.concatenate([value, value], axis=1)
+        return jnp.concatenate([pair] * (groups // 2), axis=1)
+
+    def own(rows):
+        shape = (rows, wide)
+        group = lax.broadcasted_iota(jnp.int32, shape, 0) // (rows // groups)
+        return lax.broadcasted_iota(jnp.int32, shape, 1) // entries == group
+
+    def as_row(value):
+        return jnp.sum(jnp.where(own(groups), spread(value), 0.0), axis=0, keepdims=True)
+
+    own_chan = own(chan)
+
+    def diagonal_blocks(name):
+        weight = v[name][...].astype(f32).reshape(chan, entries)
+        return jnp.where(own_chan, spread(weight), 0.0)
+
+    for name in SMALL:
         wait(name)
-    diagonal = lax.broadcasted_iota(jnp.int32, (groups, groups), 0)
-    diagonal = diagonal == lax.broadcasted_iota(jnp.int32, (groups, groups), 1)
-    log_step = jnp.sum(jnp.where(diagonal, v["log_step"][...], 0.0), axis=1, keepdims=True)
+    normed = rms_scale(v["tokens"][...], v["mix_gain"][...])
+    drive = jnp.dot(normed, v["w_in"][...], preferred_element_type=f32).astype(bf16)
+    eye = lax.broadcasted_iota(jnp.int32, (groups, groups), 0)
+    eye = eye == lax.broadcasted_iota(jnp.int32, (groups, groups), 1)
+    log_step = jnp.sum(jnp.where(eye, v["log_step"][...], 0.0), axis=1, keepdims=True)
     step = jnp.exp(log_step)
     decay = v["decay"][...]
     freq = v["freq"][...]
@@ -95,63 +119,48 @@
     denom = decay * decay + freq * freq
     coef_re = ((turn_re - 1.0) * decay + turn_im * freq) / denom
     coef_im = (turn_im * decay - (turn_re - 1.0) * freq) / denom
-
-    def lane_group(shape):
-        lane = lax.broadcasted_iota(jnp.int32, shape, len(shape) - 1)
-        first = lax.broadcasted_iota(jnp.int32, shape, 0) * places
-        return (lane >= first) & (lane < first + places)
-
-    wait("tokens")
-    wait("mix_gain")
-    normed = rms_scale(v["tokens"][...], v["mix_gain"][...])
-    wait("w_in")
-    drive = jnp.dot(normed, v["w_in"][...], preferred_element_type=f32).astype(bf16)
-    own_group = lane_group((groups, seqs, chan))
-    apart = jnp.where(own_group, drive.astype(f32)[None], 0.0).astype(bf16)
-    apart = apart.reshape(groups * seqs, chan)
-
-    def driven(ref):
-        weight = ref[...].astype(f32).reshape(chan, entries).astype(bf16)
-        value = jnp.dot(apart, weight, preferred_element_type=f32)
-        return value.reshape(groups, seqs, entries)
-
-    for name in ("in_re", "in_im"):
-        wait(name)
-    drive_re, drive_im = driven(v["in_re"]), driven(v["in_im"])
-    turn_re, turn_im = turn_re[:, None, :], turn_im[:, None, :]
-    coef_re, coef_im = coef_re[:, None, :], coef_im[:, None, :]
-    drain(state_re, state_sem.at[0])
-    drain(state_im, state_sem.at[1])
-    old_re, old_im = state_re[...], state_im[...]
-    new_re = turn_re * old_re - turn_im * old_im + (coef_re * drive_re - coef_im * drive_im)
-    new_im = turn_re * old_im + turn_im * old_re + (coef_re * drive_im + coef_im * drive_re)
-    state_re[...] = new_re
-    state_im[...] = new_im
-
-    def read_out(value, ref):
-        weight = ref[...].astype(f32).reshape(chan, entries).astype(bf16)
-        value = value.reshape(groups * seqs, entries)
-        high = value.astype(bf16)
-        low = (value - high.astype(f32)).astype(bf16)
-        dims = (((1,), (1,)), ((), ()))
-        total = lax.dot_general(high, weight, dims, preferred_element_type=f32)
-        return total + lax.dot_general(low, weight, dims, preferred_element_type=f32)
-
-    for name in ("out_re", "out_im", "skip"):
-        wait(name)
-    spread = lax.broadcasted_iota(jnp.int32, (places, chan), 1) % places
-    spread = spread == lax.broadcasted_iota(jnp.int32, (places, chan), 0)
+    turn_re, turn_im, coef_re, coef_im = map(as_row, (turn_re, turn_im, coef_re, coef_im))
+
+    in_re = diagonal_blocks("in_re").astype(bf16)
+    in_im = diagonal_blocks("in_im").astype(bf16)
+
+    out_re = diagonal_blocks("out_re").astype(bf16)
+    out_im = (-diagonal_blocks("out_im")).astype(bf16)
+    out = jnp.concatenate([out_re, out_im], axis=1)
+    lane = lax.broadcasted_iota(jnp.int32, (places, chan), 1) % places
+    lane = lane == lax.broadcasted_iota(jnp.int32, (places, chan), 0)
     skip = jnp.dot(
         v["skip"][...],
-        spread.astype(f32),
+        lane.astype(f32),
         precision=lax.Precision.HIGHEST,
         preferred_element_type=f32,
     )
-    skip = jnp.sum(jnp.where(lane_group((groups, chan)), skip, 0.0), axis=0, keepdims=True)
-    read = read_out(new_re, v["out_re"]) - read_out(new_im, v["out_im"])
-    read = jnp.where(own_group, read.reshape(groups, seqs, chan), 0.0)
-    read = jnp.sum(read, axis=0) + skip * drive.astype(f32)
-    return jax.nn.gelu(read).astype(bf16)
+    group = lax.broadcasted_iota(jnp.int32, (groups, chan), 1) // places
+    group = group == lax.broadcasted_iota(jnp.int32, (groups, chan), 0)
+    skip = jnp.sum(jnp.where(group, skip, 0.0), axis=0, keepdims=True)
+    drive_re = jnp.dot(drive, in_re, preferred_element_type=f32)
+    drive_im = jnp.dot(drive, in_im, preferred_element_type=f32)
+    drain(state_re, state_sem.at[0])
+    drain(state_im, state_sem.at[1])
+    old_re = jnp.concatenate([state_re[g] for g in range(groups)], axis=1)
+    old_im = jnp.concatenate([state_im[g] for g in range(groups)], axis=1)
+    kept_re = turn_re * old_re - turn_im * old_im
+    kept_im = turn_re * old_im + turn_im * old_re
+    new_re = kept_re + (coef_re * drive_re - coef_im * drive_im)
+    new_im = kept_im + (coef_re * drive_im + coef_im * drive_re)
+    value = jnp.concatenate([new_re, new_im], axis=1)
+    high = value.astype(bf16)
+    low = (value - high.astype(f32)).astype(bf16)
+    both = jnp.concatenate([high, low], axis=0)
+    read = lax.dot_general(both, out, (((1,), (1,)), ((), ())), preferred_element_type=f32)
+    read = read[:seqs] + read[seqs:] + skip * drive.astype(f32)
+
+    def keep():
+        for g in range(groups):
+            state_re[g] = new_re[:, g * entries : (g + 1) * entries]
+            state_im[g] = new_im[:, g * entries : (g + 1) * entries]
+
+    return jax.nn.gelu(read).astype(bf16), keep
 
 
 def gated_unit(gate, up):
@@ -203,8 +212,8 @@
     slots = n_ep * slot_rows
     hidden_n = v["gate"].shape[1]
     peers = tuple(range(n_tp - 1, 0, -1))
-    chunks = chunks_of(n_ep)
-    first_part = [start for start, _ in chunks].index(0)
+    parts = groups_of(n_ep)
+    own_place, partner = n_ep - 2, n_ep - 1
 
     def copy_of(name):
         src = hbm[name]
@@ -246,12 +255,13 @@
     def ep_peer(i):
         return paired(ep, offset_at(i, n_ep), n_ep)
 
-    mixed = mixer(v, wait, state_re, state_im, state_sem)
+    mixed, keep = mixer(v, wait, state_re, state_im, state_sem)
     mixed_ref[...] = mixed
     pl.semaphore_wait(barrier, n_tp + n_ep - 2)
     for k in peers:
         remote(mixed_ref, ag_buf.at[k - 1], ag_s.at[k - 1], ag_r.at[k - 1], "tp", tp_peer(k))
 
+    keep()
     def one_hot(index, size):
         return lax.broadcasted_iota(jnp.int32, (seqs, size), 1).astype(f32) == index
 
@@ -315,33 +325,39 @@
 
     def dispatch(i):
         to = ep_peer(i)
-        remote(disp.at[to], rows.at[tp, i], disp_s, disp_r.at[i - 1], "ep", to)
-
-    each(1, n_ep, dispatch)
-
-    for k in peers:
-        remote(disp.at[ep], rows.at[tp, 0], fwd_s.at[k - 1], fwd_r.at[first_part, k - 1], "tp", tp_peer(k))
-    rows[tp, 0] = disp[ep]
-
-    for start, part, count in sorted((start, part, count) for part, (start, count) in enumerate(chunks)):
-
-        def forward(i, part=part):
-            here = rows.at[tp, i]
-            drain(here, disp_r.at[i - 1])
-            for k in peers:
-                remote(here, here, fwd_s.at[k - 1], fwd_r.at[part, k - 1], "tp", tp_peer(k))
-
-        each(max(start, 1), start + count, forward)
-
-    for part, (start, count) in enumerate(chunks):
+        remote(disp.at[to], rows.at[tp, i], disp_s, disp_r.at[i], "ep", to)
+
+    dispatch(partner)
+    each(0, own_place, dispatch)
+
+    def pass_on(i, here):
+        for k in peers:
+            remote(here, rows.at[tp, i], fwd_s.at[k - 1], fwd_r.at[i, k - 1], "tp", tp_peer(k))
+
+    pass_on(own_place, disp.at[ep])
+    rows[tp, own_place] = disp[ep]
+
+    def forward(i):
+        here = rows.at[tp, i]
+        drain(here, disp_r.at[i])
+        pass_on(i, here)
+
+    forward(partner)
+    each(0, own_place, forward)
+
+    for part, members in enumerate(PASSES):
+        start, count = parts[members[0]][0], sum(parts[member][1] for member in members)
         span = pl.ds(start, count)
         held = xn.at[pl.ds(0, count * slot_rows)]
 
         def row_values(owner):
             return rows[owner, span].astype(f32).reshape(count * slot_rows, width)
 
-        for k in reversed(peers):
-            drain(rows.at[tp_peer(k), span], fwd_r.at[part, k - 1])
+        def landed(i):
+            for k in reversed(peers):
+                drain(rows.at[tp_peer(k), i], fwd_r.at[i, k - 1])
+
+        each(start, start + count, landed)
         squares = sum(row_values(owner) * row_values(owner) for owner in range(n_tp))
         squares = jnp.sum(squares, axis=1, keepdims=True)
         scale = lax.rsqrt(squares / (n_tp * width) + norm_eps)
@@ -363,28 +379,35 @@
             value = jnp.dot(hidden, v["down"][:, columns(owner)], preferred_element_type=f32)
             return value.reshape(count, blocks, 8, width).astype(bf16)
 
-        def give_back(k, value):
-            back_out[k - 1, span] = value
+        def give_back(member, k):
+            where = pl.ds(*parts[member])
             remote(
-                back_out.at[k - 1, span],
-                back_in.at[k - 1, span],
-                back_s.at[k - 1],
-                back_r.at[part, k - 1],
+                back_out.at[k - 1, where],
+                back_in.at[k - 1, where],
+                back_s.at[member, k - 1],
+                back_r.at[member, k - 1],
                 "tp",
                 tp_peer(k),
             )
+
+        def hand(k, value):
+            back_out[k - 1, span] = value
+            give_back(members[0], k)
 
         ready = None
         for k in peers:
             value = down(tp_peer(k))
             if ready is not None:
-                give_back(*ready)
+                hand(*ready)
             ready = k, value
         own = down(tp)
-        give_back(*ready)
+        hand(*ready)
+        for member in members[1:]:
+            for k in peers:
+                give_back(member, k)
         back_own[span] = own
 
-    for part, (start, count) in enumerate(chunks):
+    for part, (start, count) in enumerate(parts):
         for k in peers:
             drain(back_in.at[k - 1, pl.ds(start, count)], back_r.at[part, k - 1])
 
@@ -393,21 +416,23 @@
             for k in reversed(peers):
                 result += back_in[k - 1, i].astype(f32)
             result = result.astype(bf16)
-            if isinstance(i, int) and i == 0:
+            if isinstance(i, int) and i == own_place:
                 ret_in[ep] = result
                 return
             to = ep_peer(i)
             ret_out[to] = result
-            remote(ret_out.at[to], ret_in.at[ep], ret_s, ret_r.at[i - 1], "ep", to)
-
-        if start == 0:
-            settle(0)
-        each(max(start, 1), start + count, settle)
+            remote(ret_out.at[to], ret_in.at[ep], ret_s, ret_r.at[i], "ep", to)
+
+        each(start, min(start + count, own_place), settle)
+        if start + count == n_ep:
+            settle(partner)
+            settle(own_place)
 
     def arrived(i):
-        drain(ret_in.at[ep_peer(i)], ret_r.at[i - 1])
-
-    each(1, n_ep, arrived)
+        drain(ret_in.at[ep_peer(i)], ret_r.at[i])
+
+    each(0, own_place, arrived)
+    arrived(partner)
 
     returned = ret_in[...].astype(f32).reshape(slots, width).astype(bf16)
     high = combine.astype(bf16)
@@ -420,7 +445,8 @@
         drain(mixed_ref, ag_s.at[k - 1])
         drain(rs_out.at[k - 1], rs_s.at[k - 1])
         drain(rows.at[0], fwd_s.at[k - 1])
-        drain(back_out.at[k - 1], back_s.at[k - 1])
+        for part, where in enumerate(parts):
+            drain(back_out.at[k - 1, pl.ds(*where)], back_s.at[part, k - 1])
     drain(disp.at[pl.ds(0, n_ep - 1)], disp_s)
     drain(ret_out.at[pl.ds(0, n_ep - 1)], ret_s)
 
@@ -473,7 +499,7 @@
     chan = w_in.shape[1]
     state_block = (decay_re.shape[0], seq_count, state_re.shape[2])
     block = (slot_rows // 8, 8, local_width)
-    chunks = chunks_of(experts)
+    most = max(sum(groups_of(experts)[part][1] for part in members) for members in PASSES)
     bf16 = jnp.bfloat16
     dma = pltpu.SemaphoreType.DMA
     vmem = pl.BlockSpec(memory_space=pltpu.VMEM)
@@ -522,7 +548,7 @@
             pltpu.VMEM((n_tp - 1, seq_count, local_width), bf16),
             pltpu.VMEM((experts,) + block, bf16),
             pltpu.VMEM((n_tp, experts) + block, bf16),
-            pltpu.VMEM((max(c for _, c in chunks) * slot_rows, model_width), bf16),
+            pltpu.VMEM((most * slot_rows, model_width), bf16),
             pltpu.VMEM((n_tp - 1, experts) + block, bf16),
             pltpu.VMEM((experts,) + block, bf16),
             pltpu.VMEM((n_tp - 1, experts) + block, bf16),
@@ -535,13 +561,13 @@
             dma((n_tp - 1,)),
             dma((n_tp - 1,)),
             dma,
-            dma((experts - 1,)),
+            dma((experts,)),
             dma((n_tp - 1,)),
-            dma((len(chunks), n_tp - 1)),
-            dma((n_tp - 1,)),
-            dma((len(chunks), n_tp - 1)),
+            dma((experts, n_tp - 1)),
+            dma((4, n_tp - 1)),
+            dma((4, n_tp - 1)),
             dma,
-            dma((experts - 1,)),
+            dma((experts,)),
         ],
         compiler_params=pltpu.CompilerParams(
             collective_id=0, has_side_effects=True, vmem_limit_bytes=58 * 1024 * 1024

time: 40 us -> 38.6 us (0.965)
  Pallas kernels: 39.2 us -> 37.7 us
    pallas_call x1, Pallas kernels: 38.2 us -> 36.7 us  [local(): pl.pallas_call(functools.partial(layer, n_tp, experts), out_shape=(pltpu....]
where the time goes in v3:
time: 38.6 us; the launch traced here: 38.4 us
  Pallas kernels  37.7 us (98%)
  between operations  0.65 us (2%)
    pallas_call x1, Pallas kernels, local(): pl.pallas_call(functools.partial(layer, n_tp, experts), out_shape=(pltpu....  36.7 us
    pallas_call x1, Pallas kernels, local(): pl.pallas_call(store, out_shape=(jax.ShapeDtypeStruct((seq_count, local_w...  0.99 us

profile of v3, /device:TPU:0, one launch (start us, length us, event | category | flops | bytes accessed | tf_op | source)
XLA Modules:
  0.0 38.4 jit_solution(16070863350087196011)
XLA Ops:
  0.6 36.7 %shard_map.229 = (bf16[64,512]{1,0:T(8,128)(2,1)S(1)}, f32[16,64,64]{2,1,0:T(8,128)S(1)}, f32[16,64,64]{2,1,0:T(8,128)S(1)}) custom-call(bf16[64,2048]{1,0:T(8,128)(2,1)} %refs_0_.1, bf16[2048,256]{1,0:T(8,128)(2,1)} %refs_1_.1, f32[1,2048]{1,0:T(1,128)} %bitcast.6, f32[16,64]{1,0:T(8,128)} %refs_3_.1, f32[16,64]{1,0:T(8,128)} %refs_4_.1, f32[1,16]{1,0:T(1,128)} %bitcast.11, ...), custom_call_target="tpu_custom_call" | custom-call | tf_op jit(solution)/shard_map/pallas_call | solution.py:534
  37.4 1.0 %shard_map.230 = (bf16[64,512]{1,0:T(8,128)(2,1)}, f32[64,16,64]{2,1,0:T(8,128)}, f32[64,16,64]{2,1,0:T(8,128)}) custom-call(bf16[64,512]{1,0:T(8,128)(2,1)S(1)} %get-tuple-element.6.mixed_ref, f32[16,64,64]{2,1,0:T(8,128)S(1)} %get-tuple-element.7.re_ref, f32[16,64,64]{2,1,0:T(8,128)S(1)} %get-tuple-element.8.im_ref), custom_call_target="tpu_custom_call" | custom-call | tf_op jit(solution)/shard_map/pallas_call | solution.py:577

commit v4 on v3

--- a/solution.py
+++ b/solution.py
@@ -103,9 +103,12 @@
         weight = v[name][...].astype(f32).reshape(chan, entries)
         return jnp.where(own_chan, spread(weight), 0.0)
 
+    wait("tokens")
+    wait("mix_gain")
+    normed = rms_scale(v["tokens"][...], v["mix_gain"][...])
     for name in SMALL:
-        wait(name)
-    normed = rms_scale(v["tokens"][...], v["mix_gain"][...])
+        if name not in ("tokens", "mix_gain"):
+            wait(name)
     drive = jnp.dot(normed, v["w_in"][...], preferred_element_type=f32).astype(bf16)
     eye = lax.broadcasted_iota(jnp.int32, (groups, groups), 0)
     eye = eye == lax.broadcasted_iota(jnp.int32, (groups, groups), 1)
@@ -286,6 +289,7 @@
         pick = one_hot(choice * slot_rows + rank, slots)
         select = jnp.where(pick, 1.0, select)
         combine = jnp.where(pick, upright(weight_ref, k), combine)
+    select = select.T.astype(bf16)
 
     def glu_rows(owner):
         return v["glu"][pl.ds(pl.multiple_of(owner * chan, chan), chan), :]
@@ -318,9 +322,7 @@
         total += rs_in[k - 1].astype(f32)
     resid = (v["tokens"][:, columns(tp)].astype(f32) + total).astype(bf16)
 
-    picked = lax.dot_general(
-        select.astype(bf16), resid, (((0,), (0,)), ((), ())), preferred_element_type=f32
-    )
+    picked = jnp.dot(select, resid, preferred_element_type=f32)
     disp[...] = picked.reshape(n_ep, blocks, 8, width).astype(bf16)
 
     def dispatch(i):
@@ -437,9 +439,9 @@
     returned = ret_in[...].astype(f32).reshape(slots, width).astype(bf16)
     high = combine.astype(bf16)
     low = (combine - high.astype(f32)).astype(bf16)
-    expert_total = jnp.dot(high, returned, preferred_element_type=f32)
-    expert_total += jnp.dot(low, returned, preferred_element_type=f32)
-    out_ref[...] = (resid.astype(f32) + expert_total).astype(bf16)
+    both = jnp.concatenate([high, low], axis=0)
+    both = jnp.dot(both, returned, preferred_element_type=f32)
+    out_ref[...] = (resid.astype(f32) + (both[:seqs] + both[seqs:])).astype(bf16)
 
     for k in peers:
         drain(mixed_ref, ag_s.at[k - 1])

time: 38.6 us -> 38.5 us (level)
  no operation moved by 1% of the time
where the time goes in v4:
time: 38.5 us; the launch traced here: 38.3 us
  Pallas kernels  37.6 us (98%)
  between operations  0.65 us (2%)
    pallas_call x1, Pallas kernels, local(): pl.pallas_call(functools.partial(layer, n_tp, experts), out_shape=(pltpu....  36.6 us
    pallas_call x1, Pallas kernels, local(): pl.pallas_call(store, out_shape=(jax.ShapeDtypeStruct((seq_count, local_w...  0.99 us

profile of v4, /device:TPU:0, one launch (start us, length us, event | category | flops | bytes accessed | tf_op | source)
XLA Modules:
  0.0 38.3 jit_solution(7058393577874758675)
XLA Ops:
  0.6 36.6 %shard_map.229 = (bf16[64,512]{1,0:T(8,128)(2,1)S(1)}, f32[16,64,64]{2,1,0:T(8,128)S(1)}, f32[16,64,64]{2,1,0:T(8,128)S(1)}) custom-call(bf16[64,2048]{1,0:T(8,128)(2,1)} %refs_0_.1, bf16[2048,256]{1,0:T(8,128)(2,1)} %refs_1_.1, f32[1,2048]{1,0:T(1,128)} %bitcast.6, f32[16,64]{1,0:T(8,128)} %refs_3_.1, f32[16,64]{1,0:T(8,128)} %refs_4_.1, f32[1,16]{1,0:T(1,128)} %bitcast.11, ...), custom_call_target="tpu_custom_call" | custom-call | tf_op jit(solution)/shard_map/pallas_call | solution.py:536
  37.3 1.0 %shard_map.230 = (bf16[64,512]{1,0:T(8,128)(2,1)}, f32[64,16,64]{2,1,0:T(8,128)}, f32[64,16,64]{2,1,0:T(8,128)}) custom-call(bf16[64,512]{1,0:T(8,128)(2,1)S(1)} %get-tuple-element.6.mixed_ref, f32[16,64,64]{2,1,0:T(8,128)S(1)} %get-tuple-element.7.re_ref, f32[16,64,64]{2,1,0:T(8,128)S(1)} %get-tuple-element.8.im_ref), custom_call_target="tpu_custom_call" | custom-call | tf_op jit(solution)/shard_map/pallas_call | solution.py:579
